TPU v7x, 32 devices: a whole 2x2x4 slice. The times are simulated.
32 devices in a mesh: ep: 8 (over z, x), tp: 4 (over y, core).
Axes of the slice: x: 2, y: 2, z: 4, core: 2. Of those that a mesh axis runs over, the one named last changes fastest.
Arguments:
- mixer_rows: bfloat16 [1024, 2048], P('ep'), may hold values from -40 to 40
- mixer_gain: float32 [2048], replicated, may hold values from 0.1 to 1.9
- inner_weight: bfloat16 [2048, 1024], P(None, 'tp'), may hold values from -0.125 to 0.125
- gate_in_weight: bfloat16 [2048, 1024], P(None, 'tp'), may hold values from -0.125 to 0.125
- gate_out_weight: bfloat16 [2048, 1024], P(None, 'tp'), may hold values from -0.125 to 0.125
- conv_taps: float32 [3, 1024], P(None, 'tp'), may hold values from -3.5 to 3.5
- mixer_out_weight: bfloat16 [1024, 2048], P('tp'), may hold values from -0.1875 to 0.1875
- routed_rows: bfloat16 [2048, 2048], P('ep'), may hold values from -40 to 40
- routed_gain: float32 [2048], replicated, may hold values from 0.1 to 1.9
- route_ids: int32 [2048, 2], P('ep'), may hold values from 0 to 7, all different within a row; in each aligned block of 256 rows (0 to 255, 256 to 511, ...) at most 128 rows name the same one
- route_weights: float32 [2048, 2], P('ep'), may hold values from 0.25 to 1
- expert_gate: bfloat16 [8, 2048, 2048], P('ep', None, 'tp'), may hold values from -0.125 to 0.125
- expert_up: bfloat16 [8, 2048, 2048], P('ep', None, 'tp'), may hold values from -0.125 to 0.125
- expert_down: bfloat16 [8, 2048, 2048], P('ep', 'tp'), may hold values from -0.125 to 0.125
Outputs:
- mixer_output: bfloat16 [1024, 2048], P('ep')
- routed_output: bfloat16 [2048, 2048], P('ep')
Inputs may be any that keep to these rules, and one draw needn't show every extreme that they name: `route_ids`: within each aligned block of 256 tokens, no expert is named by more than 128 choices, a bound that some block reaches; a token's 2 experts differ.
All inputs are finite; a program needn't handle non-finite values.
Results may differ from a plain program's by a relative error of at most 0.019.
Values may be sent and summed in bfloat16 or wider, within the bound.
A program may use at most 64 MiB of HBM per device.

v0:
```python
import jax
import jax.numpy as jnp
from jax import lax
from jax.sharding import PartitionSpec as P


def shifted(value, axis, steps):
    count = lax.axis_size(axis)
    initial, last = (max(0, -steps), min(count, count - steps))
    return lax.ppermute(value, axis, [(source, source + steps) for source in range(initial, last)])


def rms_scale(row_block, gain_row):
    values = row_block.astype(jnp.float32)
    scaled = values * lax.rsqrt(jnp.mean(values * values, axis=-1, keepdims=True) + 1e-06)
    return (scaled * gain_row).astype(jnp.bfloat16)


def on_device(
    mixer_rows,
    mixer_gain,
    inner_weight,
    gate_in_weight,
    gate_out_weight,
    conv_taps,
    mixer_out_weight,
    routed_rows,
    routed_gain,
    route_ids,
    route_weights,
    expert_gate,
    expert_up,
    expert_down,
):
    normed = rms_scale(mixer_rows, mixer_gain)
    inner_proj = jnp.dot(normed, inner_weight, preferred_element_type=jnp.float32)
    gate_in = jnp.dot(normed, gate_in_weight, preferred_element_type=jnp.float32)
    conv_input = (gate_in * inner_proj).astype(jnp.bfloat16)
    gate_out = jnp.dot(normed, gate_out_weight, preferred_element_type=jnp.float32)
    tap_total = conv_taps.shape[0]
    rim_rows = tap_total - 1
    earlier_rows = shifted(conv_input[conv_input.shape[0] - rim_rows :], "ep", 1)
    extended = jnp.concatenate([earlier_rows, conv_input], axis=0).astype(jnp.float32)
    length = conv_input.shape[0]
    conv_out = jnp.zeros(conv_input.shape, jnp.float32)
    for tap_index in range(tap_total):
        conv_out = conv_out + conv_taps[tap_index] * extended[tap_index : tap_index + length]
    gated_conv = (gate_out * conv_out).astype(jnp.bfloat16)
    mixer_terms = jnp.dot(gated_conv, mixer_out_weight, preferred_element_type=jnp.float32)
    routed_normed = rms_scale(routed_rows, routed_gain)
    experts = lax.axis_size("ep")
    groups = lax.axis_size("tp")
    column = lax.axis_index("tp")
    tok_count, pick_count = route_ids.shape
    model_width = routed_rows.shape[1]
    capacity = 2 * tok_count * pick_count // experts
    share_rows = capacity // groups
    flat_ids = route_ids.reshape(-1)
    onehot = (flat_ids[:, None] == jnp.arange(experts, dtype=jnp.int32)[None, :]).astype(jnp.int32)
    slot_rank = jnp.sum((jnp.cumsum(onehot, axis=0) - onehot) * onehot, axis=1)
    slot_number = slot_rank * experts + flat_ids
    owners = jnp.arange(tok_count * pick_count, dtype=jnp.int32) // pick_count
    matches = slot_number[None, :] == jnp.arange(capacity * experts, dtype=jnp.int32)[:, None]
    token_table = jnp.where(
        jnp.any(matches, axis=1), jnp.sum(jnp.where(matches, owners[None, :], 0), axis=1), tok_count
    )
    padded_rows = jnp.concatenate(
        [routed_normed, jnp.zeros((1, model_width), jnp.bfloat16)], axis=0
    )
    table_share = lax.dynamic_slice_in_dim(
        token_table.reshape(capacity, experts), column * share_rows, share_rows, 0
    )
    outgoing = jnp.take(padded_rows, table_share.reshape(-1), axis=0).reshape(
        share_rows, experts, model_width
    )
    arrived = lax.all_to_all(outgoing, "ep", split_axis=1, concat_axis=1, tiled=True)
    incoming = lax.all_gather(arrived, "tp", axis=0, tiled=True)
    slot_rows = incoming.reshape(capacity * experts, model_width)
    gate_act = jnp.dot(slot_rows, expert_gate[0], preferred_element_type=jnp.float32)
    up_act = jnp.dot(slot_rows, expert_up[0], preferred_element_type=jnp.float32)
    hidden = (jax.nn.silu(gate_act) * up_act).astype(jnp.bfloat16)
    summed = lax.psum_scatter(
        jnp.dot(hidden, expert_down[0], preferred_element_type=jnp.float32).astype(jnp.bfloat16),
        "tp",
        scatter_dimension=0,
        tiled=True,
    )
    returned = lax.all_to_all(
        summed.reshape(share_rows, experts, model_width),
        "ep",
        split_axis=1,
        concat_axis=1,
        tiled=True,
    )
    flat_back = jnp.concatenate(
        [
            returned.reshape(share_rows * experts, model_width),
            jnp.zeros((1, model_width), jnp.bfloat16),
        ],
        axis=0,
    )
    local_slot = jnp.where(
        slot_rank // share_rows == column,
        (slot_rank - column * share_rows) * experts + flat_ids,
        share_rows * experts,
    )
    contrib = (
        jnp.take(flat_back, local_slot, axis=0).astype(jnp.float32)
        * route_weights.reshape(-1)[:, None]
    )
    routed_terms = jnp.sum(contrib.reshape(tok_count, pick_count, model_width), axis=1)
    mixer_total, routed_total = (
        lax.psum(mixer_terms.astype(jnp.bfloat16), "tp").astype(jnp.float32),
        lax.psum(routed_terms.astype(jnp.bfloat16), "tp").astype(jnp.float32),
    )
    return (mixer_total.astype(jnp.bfloat16), routed_total.astype(jnp.bfloat16))


def solution(mesh):
    return jax.shard_map(
        on_device,
        mesh=mesh,
        in_specs=(
            P("ep", None),
            P(),
            P(None, "tp"),
            P(None, "tp"),
            P(None, "tp"),
            P(None, "tp"),
            P("tp", None),
            P("ep", None),
            P(),
            P("ep", None),
            P("ep", None),
            P("ep", None, "tp"),
            P("ep", None, "tp"),
            P("ep", "tp", None),
        ),
        out_specs=(P("ep", None), P("ep", None)),
        check_vma=False,
    )
```

profile of v0, /device:TPU:0, one launch (start us, length us, event | category | flops | bytes accessed | tf_op | source)
XLA Modules:
  0.0 255.2 jit_solution(8111063935972421025)
XLA Ops:
  8.5 1.1 reduce-window.6
  10.9 1.5 fusion.4
  13.6 2.3 gather_fusion
  15.9 2.4 copy_select_fusion
  18.4 32.8 %all_to_all.10 = bf16[32,8,2048]{2,0,1:T(8,128)(2,1)S(1)} all-to-all(bf16[32,8,2048]{2,0,1:T(8,128)(2,1)S(1)} %copy_select_fusion), channel_id=1, replica_groups=mesh['ep'=8,'tp'=4] {'ep'}, dimensions={1} | all-to-all | bytes 2097152 | tf_op jit(solution)/shard_map/all_to_all | solution.py:76
  51.2 1.5 copy.77
  52.8 33.6 %all-gather.2.cloned.1.call-done = bf16[128,8,2048]{2,1,0:T(8,128)(2,1)} async-done(((bf16[32,8,2048]{2,1,0:T(8,128)(2,1)}), bf16[128,8,2048]{2,1,0:T(8,128)(2,1)}) %all-gather.2.cloned.1.call-update) | async-done | bytes 4194320 | tf_op jit(solution)/shard_map/all_gather | solution.py:77
  86.4 6.6 %fusion.2 = f32[1024,512]{1,0:T(8,128)} fusion(bf16[128,8,2048]{2,1,0:T(8,128)(2,1)} %all-gather.2.cloned.1.call-done, bf16[1,2048,512]{2,1,0:T(8,128)(2,1)} %param.25), kind=kOutput, calls=%fused_computation.4 | convolution fusion | flops 2147483648 | bytes 8388608 | tf_op jit(solution)/shard_map/dot_general | solution.py:79
  93.0 10.0 %convolution_convert_fusion = bf16[1024,2048]{1,0:T(8,128)(2,1)} fusion(bf16[1,512,2048]{2,1,0:T(8,128)(2,1)S(1)} %copy-done, f32[1024,512]{1,0:T(8,128)} %fusion.2, bf16[1,2048,512]{2,1,0:T(8,128)(2,1)} %param.26, bf16[128,8,2048]{2,1,0:T(8,128)(2,1)} %all-gather.2.cloned.1.call-done), kind=kOutput, calls=%fused_computation.8 | convolution fusion | flops 4300210176 | bytes 14680064 | tf_op jit(solution)/shard_map/dot_general | solution.py:83
  103.0 1.0 copy-done.2
  104.2 43.5 %reduce-scatter.2.cloned.1.call-done = bf16[256,2048]{1,0:T(8,128)(2,1)} async-done(((bf16[1024,2048]{1,0:T(8,128)(2,1)}), bf16[256,2048]{1,0:T(8,128)(2,1)}) %reduce-scatter.2.cloned.1.call-update) | async-done | bytes 1048592 | tf_op jit(solution)/shard_map/reduce_scatter | solution.py:82
  147.7 2.8 %copy.78 = bf16[32,8,2048]{2,0,1:T(8,128)(2,1)} copy(bf16[32,8,2048]{2,1,0:T(8,128)(2,1)} %bitcast.47) | data formatting | bytes 2097152 | tf_op jit(solution)/shard_map/reshape | solution.py:89
  150.5 5.5 %all-to-all-start.1 = ((bf16[32,8,2048]{2,0,1:T(8,128)(2,1)}), bf16[32,8,2048]{2,0,1:T(8,128)(2,1)S(1)}, u32[]{:S(2)}, u32[]{:S(2)}) async-start(bf16[32,8,2048]{2,0,1:T(8,128)(2,1)} %copy.78), calls=%async_computation.2 | async-start | bytes 2097152 | tf_op jit(solution)/shard_map/all_to_all | solution.py:88
  156.1 1.7 fusion.40
  157.9 1.8 fusion.16
  159.7 4.1 %collective-permute-start = (bf16[2,256]{1,0:T(2,128)(2,1)S(1)}, bf16[2,256]{1,0:T(2,128)(2,1)S(1)}, u32[]{:S(2)}, u32[]{:S(2)}) collective-permute-start(bf16[2,256]{1,0:T(2,128)(2,1)S(1)} %slice.40), channel_id=1, source_target_pairs={{0,4},{4,8},{8,12},{12,16},{16,20},{20,24},{24,28},{1,5},{5,9},{9,... | collective-permute-start | bytes 3080 | tf_op jit(solution)/shard_map/ppermute | solution.py:10
  164.9 3.3 %convolution_convert_fusion.1 = bf16[128,2048]{1,0:T(8,128)(2,1)} fusion(bf16[256,2048]{1,0:T(8,128)(2,1)} %param.20, bf16[2048,256]{1,0:T(8,128)(2,1)} %param.18, f32[130,256]{1,0:T(8,128)S(1)} %maximum_convert_fusion, f32[256]{0:T(256)S(1)} %bitcast.51, f32[256]{0:T(256)S(1)} %bitcast.52, f32[256]{0:T(256)S(1)} %bitcast.50, bf16[128,2048]{1,0:T(8,128)(2,1)} %param.14, ...), kind=kOutput, calls=%fused_computation.11 | convolution fusion | flops 269975552 | bytes 3550720 | tf_op jit(solution)/shard_map/dot_general | solution.py:49
  168.2 13.5 %all-to-all-done.1 = bf16[32,8,2048]{2,0,1:T(8,128)(2,1)S(1)} async-done(((bf16[32,8,2048]{2,0,1:T(8,128)(2,1)}), bf16[32,8,2048]{2,0,1:T(8,128)(2,1)S(1)}, u32[]{:S(2)}, u32[]{:S(2)}) %all-to-all-start.1) | async-done | bytes 1048608 | tf_op jit(solution)/shard_map/all_to_all | solution.py:88
  182.4 3.3 %gather_fusion.1 = bf16[512,2048]{1,0:T(8,128)(2,1)} fusion(bf16[257,2048]{1,0:T(8,128)(2,1)S(1)} %concatenate.11, s32[1024]{0:T(1024)S(1)} %pad_clamp_fusion), kind=kCustom, calls=%fused_computation.1 | custom fusion | bytes 4196352 | tf_op jit(solution)/shard_map/jit(_take)/gather | solution.py:108
  185.7 4.4 %gather.15 = bf16[256,2,2048]{2,1,0:T(2,128)(2,1)} reshape(bf16[512,2048]{1,0:T(8,128)(2,1)} %gather_fusion.1) | data formatting | bytes 4194304 | tf_op jit(solution)/shard_map/jit(_take)/gather | solution.py:108
  190.1 10.8 %multiply_reduce_fusion = bf16[256,2048]{1,0:T(8,128)(2,1)} fusion(bf16[256,2,2048]{2,1,0:T(2,128)(2,1)} %gather.15, pred[256,2]{1,0:T(8,128)(4,1)S(1)} %copy.74, f32[256,2]{1,0:T(8,128)S(1)} %copy.81), kind=kLoop, calls=%fused_computation.6 | loop fusion | flops 3670016 | bytes 3148288 | tf_op jit(solution)/shard_map/reduce_sum | solution.py:111
  201.0 43.5 %all-reduce.5.cloned.1.call-done = (bf16[128,2048]{1,0:T(8,128)(2,1)}, bf16[256,2048]{1,0:T(8,128)(2,1)}) async-done(((bf16[128,2048]{1,0:T(8,128)(2,1)}, bf16[256,2048]{1,0:T(8,128)(2,1)}), (bf16[128,2048]{1,0:T(8,128)(2,1)}, bf16[256,2048]{1,0:T(8,128)(2,1)})) %all-reduce.5.cloned.1.call-update) | async-done | bytes 1572880 | tf_op jit(solution)/shard_map/psum | solution.py:113
  244.5 1.9 copy.87
  246.4 2.3 copy.88
  (56 shorter events, 5.7 us)
Async XLA Ops:
  7.2 85.8 %copy-start = (bf16[1,512,2048]{2,1,0:T(8,128)(2,1)S(1)}, bf16[1,512,2048]{2,1,0:T(8,128)(2,1)}, u32[]{:S(2)}) copy-start(bf16[1,512,2048]{2,1,0:T(8,128)(2,1)} %param.27) | copy-start | bytes 6291460
  7.2 5.3 %copy-start.1 = (bf16[256,2048]{1,0:T(8,128)(2,1)S(1)}, bf16[256,2048]{1,0:T(8,128)(2,1)}, u32[]{:S(2)}) copy-start(bf16[256,2048]{1,0:T(8,128)(2,1)} %param.21) | copy-start | bytes 3145732
  7.2 79.2 %all-gather.2.cloned.1.call-start = ((), (), s32[]{:S(2)}) async-start(), calls=%async_computation.3 | async-start | bytes 5242880 | tf_op jit(solution)/shard_map/all_gather | solution.py:77
  52.8 95.0 %reduce-scatter.2.cloned.1.call-start = ((), (), s32[]{:S(2)}) async-start(), calls=%async_computation.4 | async-start | bytes 5242880 | tf_op jit(solution)/shard_map/reduce_scatter | solution.py:82
  103.0 1.0 copy-start.2
  147.7 8.4 %copy-start.3 = (f32[2048]{0:T(1024)S(1)}, f32[2048]{0:T(1024)}, u32[]{:S(2)}) copy-start(f32[2048]{0:T(1024)} %param.15) | copy-start | bytes 24580
  150.5 31.2 %all-to-all-start.1 = ((bf16[32,8,2048]{2,0,1:T(8,128)(2,1)}), bf16[32,8,2048]{2,0,1:T(8,128)(2,1)S(1)}, u32[]{:S(2)}, u32[]{:S(2)}) async-start(bf16[32,8,2048]{2,0,1:T(8,128)(2,1)} %copy.78), calls=%async_computation.2 | async-start | bytes 2097152 | tf_op jit(solution)/shard_map/all_to_all | solution.py:88
  156.0 8.1 %copy-start.4 = (s32[256,2]{0,1:T(2,128)S(1)}, s32[256,2]{0,1:T(2,128)}, u32[]{:S(2)}) copy-start(s32[256,2]{0,1:T(2,128)} %param.23) | copy-start | bytes 6148
  156.0 8.1 %copy-start.5 = (f32[3,256]{1,0:T(4,128)S(1)}, f32[3,256]{1,0:T(4,128)}, u32[]{:S(2)}) copy-start(f32[3,256]{1,0:T(4,128)} %param.19) | copy-start | bytes 9220
  156.0 88.4 %all-reduce.5.cloned.1.call-start = ((), (), s32[]{:S(2)}) async-start(), calls=%async_computation.5 | async-start | bytes 3145728 | tf_op jit(solution)/shard_map/psum | solution.py:113
  156.1 8.3 %copy-start.6 = (f32[256,2]{0,1:T(2,128)S(1)}, f32[256,2]{0,1:T(2,128)}, u32[]{:S(2)}) copy-start(f32[256,2]{0,1:T(2,128)} %param.24) | copy-start | bytes 6148
  159.7 5.2 %collective-permute-start = (bf16[2,256]{1,0:T(2,128)(2,1)S(1)}, bf16[2,256]{1,0:T(2,128)(2,1)S(1)}, u32[]{:S(2)}, u32[]{:S(2)}) collective-permute-start(bf16[2,256]{1,0:T(2,128)(2,1)S(1)} %slice.40), channel_id=1, source_target_pairs={{0,4},{4,8},{8,12},{12,16},{16,20},{20,24},{24,28},{1,5},{5,9},{9,... | collective-permute-start | bytes 3080 | tf_op jit(solution)/shard_map/ppermute | solution.py:10
Sparse Core Ops, SparseCore 0:
  52.9 33.4 all-gather.1
  103.1 44.5 reduce-scatter.1
  201.1 43.3 all-reduce.4
where the time goes:
time: 256 us; the launch traced here: 255 us
  waiting for transfers between devices  134 us (52%)
  blocking collectives  32.8 us (13%)
  matrix products  23.4 us (9%)
  local copies, waits for them, and re-layouts  22.8 us (9%)
  other arithmetic  18 us (7%)
  between operations  14 us (5%)
  starting transfers between devices  9.73 us (4%)
    reduce_scatter x1, waiting for transfers between devices, on_device(): lax.psum_scatter(jnp.dot(hidden, expert_down[0], preferred_element_type=j...  43.5 us
    psum x1, waiting for transfers between devices, on_device(): lax.psum(mixer_terms.astype(jnp.bfloat16), 'tp').astype(jnp.float32)  43.5 us
    all_gather x1, waiting for transfers between devices, on_device(): incoming = lax.all_gather(arrived, 'tp', axis=0, tiled=True)  33.6 us
    all_to_all x1, blocking collectives, on_device(): lax.all_to_all(outgoing, 'ep', split_axis=1, concat_axis=1, tiled=True)  32.8 us
    all_to_all x1, waiting for transfers between devices, on_device(): lax.all_to_all(summed.reshape(share_rows, experts, model_width), 'ep', sp...  13.5 us
    reduce_sum x1, other arithmetic, on_device(): jnp.sum(contrib.reshape(tok_count, pick_count, model_width), axis=1)  10.8 us
    dot_general x1, matrix products, on_device(): jnp.dot(hidden, expert_down[0], preferred_element_type=jnp.float32)  9.96 us
    gather x2, local copies, waits for them, and re-layouts, on_device(): jnp.take(flat_back, local_slot, axis=0).astype(jnp.float32)  7.75 us
  transfers between devices with their start and end apart: 5, of which 5 were waited for; matrix products, arithmetic and copies ran while one was open for 3% of the time, Pallas kernels for 0%

commit v1 on v0

--- a/solution.py
+++ b/solution.py
@@ -110,7 +110,7 @@
     )
     routed_terms = jnp.sum(contrib.reshape(tok_count, pick_count, model_width), axis=1)
     mixer_total, routed_total = (
-        lax.psum(mixer_terms.astype(jnp.bfloat16), "tp").astype(jnp.float32),
+        jnp.sum(lax.all_gather(mixer_terms.astype(jnp.bfloat16), "tp"), axis=0).astype(jnp.float32),
         lax.psum(routed_terms.astype(jnp.bfloat16), "tp").astype(jnp.float32),
     )
     return (mixer_total.astype(jnp.bfloat16), routed_total.astype(jnp.bfloat16))

time: 256 us -> 245 us (0.957)
  waiting for transfers between devices: 134 us -> 124 us
  other arithmetic: 18 us -> 20.9 us
    psum x1, waiting for transfers between devices: 43.5 us -> 31.5 us  [on_device(): lax.psum(routed_terms.astype(jnp.bfloat16), 'tp').astype(jnp.float32)]
    all_to_all x1, waiting for transfers between devices: 13.5 us -> 24.8 us  [on_device(): lax.all_to_all(summed.reshape(share_rows, experts, model_width), 'ep', sp...]
    reduce_scatter x1, waiting for transfers between devices: 43.5 us -> 33 us  [on_device(): lax.psum_scatter(jnp.dot(hidden, expert_down[0], preferred_element_type=j...]
    reduce_sum x0 -> x1, other arithmetic: none -> 2.92 us  [on_device(): jnp.sum(lax.all_gather(mixer_terms.astype(jnp.bfloat16), 'tp'), axis=0)]
    unnamed x18 -> x19, local copies, waits for them, and re-layouts: 6.36 us -> 4.41 us
  transfers between devices with their start and end apart: 5 -> 6, of which waited for: 5 -> 5; matrix products, arithmetic and copies ran while one was open for 3% -> 13% of each run, Pallas kernels for 0% -> 0%
where the time goes in v1:
time: 245 us; the launch traced here: 244 us
  waiting for transfers between devices  124 us (51%)
  blocking collectives  32.8 us (13%)
  matrix products  22.3 us (9%)
  local copies, waits for them, and re-layouts  20.9 us (9%)
  other arithmetic  20.9 us (9%)
  between operations  14 us (6%)
  starting transfers between devices  9.05 us (4%)
    all_gather x1, waiting for transfers between devices, on_device(): incoming = lax.all_gather(arrived, 'tp', axis=0, tiled=True)  33.6 us
    reduce_scatter x1, waiting for transfers between devices, on_device(): lax.psum_scatter(jnp.dot(hidden, expert_down[0], preferred_element_type=j...  33 us
    all_to_all x1, blocking collectives, on_device(): lax.all_to_all(outgoing, 'ep', split_axis=1, concat_axis=1, tiled=True)  32.8 us
    psum x1, waiting for transfers between devices, on_device(): lax.psum(routed_terms.astype(jnp.bfloat16), 'tp').astype(jnp.float32)  31.5 us
    all_to_all x1, waiting for transfers between devices, on_device(): lax.all_to_all(summed.reshape(share_rows, experts, model_width), 'ep', sp...  24.8 us
    reduce_sum x1, other arithmetic, on_device(): jnp.sum(contrib.reshape(tok_count, pick_count, model_width), axis=1)  10.8 us
    dot_general x1, matrix products, on_device(): jnp.dot(hidden, expert_down[0], preferred_element_type=jnp.float32)  9.96 us
    gather x2, local copies, waits for them, and re-layouts, on_device(): jnp.take(flat_back, local_slot, axis=0).astype(jnp.float32)  7.75 us
  transfers between devices with their start and end apart: 6, of which 5 were waited for; matrix products, arithmetic and copies ran while one was open for 13% of the time, Pallas kernels for 0%

profile of v1, /device:TPU:0, one launch (start us, length us, event | category | flops | bytes accessed | tf_op | source)
XLA Modules:
  0.0 244.3 jit_solution(13137648703598323531)
XLA Ops:
  8.5 1.1 reduce-window.6
  10.9 1.5 fusion.4
  12.5 1.0 fusion.6
  13.6 2.3 gather_fusion
  15.9 2.4 %copy_select_fusion = bf16[32,8,2048]{2,0,1:T(8,128)(2,1)S(1)} fusion(bf16[32,8,2048]{2,1,0:T(8,128)(2,1)} %bitcast.46, pred[32,8]{0,1:T(8,128)(4,1)S(1)} %copy.75), kind=kLoop, calls=%fused_computation.32 | loop fusion | flops 524288 | bytes 2097408 | tf_op jit(solution)/shard_map/jit(_take)/select_n | solution.py:73
  18.4 32.8 %all_to_all.10 = bf16[32,8,2048]{2,0,1:T(8,128)(2,1)S(1)} all-to-all(bf16[32,8,2048]{2,0,1:T(8,128)(2,1)S(1)} %copy_select_fusion), channel_id=1, replica_groups=mesh['ep'=8,'tp'=4] {'ep'}, dimensions={1} | all-to-all | bytes 2097152 | tf_op jit(solution)/shard_map/all_to_all | solution.py:76
  51.2 1.5 copy.77
  52.8 33.6 %all-gather.4.cloned.1.call-done = bf16[128,8,2048]{2,1,0:T(8,128)(2,1)} async-done(((bf16[32,8,2048]{2,1,0:T(8,128)(2,1)}), bf16[128,8,2048]{2,1,0:T(8,128)(2,1)}) %all-gather.4.cloned.1.call-update) | async-done | bytes 4194320 | tf_op jit(solution)/shard_map/all_gather | solution.py:77
  86.4 6.6 %fusion.2 = f32[1024,512]{1,0:T(8,128)} fusion(bf16[128,8,2048]{2,1,0:T(8,128)(2,1)} %all-gather.4.cloned.1.call-done, bf16[1,2048,512]{2,1,0:T(8,128)(2,1)} %param.25), kind=kOutput, calls=%fused_computation.4 | convolution fusion | flops 2147483648 | bytes 8388608 | tf_op jit(solution)/shard_map/dot_general | solution.py:79
  93.0 10.0 %convolution_convert_fusion = bf16[1024,2048]{1,0:T(8,128)(2,1)} fusion(bf16[1,512,2048]{2,1,0:T(8,128)(2,1)S(1)} %copy-done, f32[1024,512]{1,0:T(8,128)} %fusion.2, bf16[1,2048,512]{2,1,0:T(8,128)(2,1)} %param.26, bf16[128,8,2048]{2,1,0:T(8,128)(2,1)} %all-gather.4.cloned.1.call-done), kind=kOutput, calls=%fused_computation.8 | convolution fusion | flops 4300210176 | bytes 14680064 | tf_op jit(solution)/shard_map/dot_general | solution.py:83
  104.2 1.7 fusion.40
  106.3 3.4 %collective-permute-start = (bf16[2,256]{1,0:T(2,128)(2,1)S(1)}, bf16[2,256]{1,0:T(2,128)(2,1)S(1)}, u32[]{:S(2)}, u32[]{:S(2)}) collective-permute-start(bf16[2,256]{1,0:T(2,128)(2,1)S(1)} %slice.40), channel_id=1, source_target_pairs={{0,4},{4,8},{8,12},{12,16},{16,20},{20,24},{24,28},{1,5},{5,9},{9,... | collective-permute-start | bytes 3080 | tf_op jit(solution)/shard_map/ppermute | solution.py:10
  109.7 1.3 collective-permute-done
  111.0 3.7 %convolution_convert_fusion.1 = bf16[128,2048]{1,0:T(8,128)(2,1)} fusion(bf16[256,2048]{1,0:T(8,128)(2,1)} %param.20, bf16[2048,256]{1,0:T(8,128)(2,1)} %param.18, f32[130,256]{1,0:T(8,128)S(1)} %maximum_convert_fusion, f32[256]{0:T(256)S(1)} %bitcast.53, f32[256]{0:T(256)S(1)} %bitcast.54, f32[256]{0:T(256)S(1)} %bitcast.52, ...), kind=kOutput, calls=%fused_computation.11 | convolution fusion | flops 269975552 | bytes 3550720 | tf_op jit(solution)/shard_map/dot_general | solution.py:49
  114.7 33.0 %reduce-scatter.2.cloned.1.call-done = bf16[256,2048]{1,0:T(8,128)(2,1)} async-done(((bf16[1024,2048]{1,0:T(8,128)(2,1)}), bf16[256,2048]{1,0:T(8,128)(2,1)}) %reduce-scatter.2.cloned.1.call-update) | async-done | bytes 1048592 | tf_op jit(solution)/shard_map/reduce_scatter | solution.py:82
  147.7 2.8 %copy.78 = bf16[32,8,2048]{2,0,1:T(8,128)(2,1)} copy(bf16[32,8,2048]{2,1,0:T(8,128)(2,1)} %bitcast.49) | data formatting | bytes 2097152 | tf_op jit(solution)/shard_map/reshape | solution.py:89
  150.5 5.5 %all-to-all-start.1 = ((bf16[32,8,2048]{2,0,1:T(8,128)(2,1)}), bf16[32,8,2048]{2,0,1:T(8,128)(2,1)S(1)}, u32[]{:S(2)}, u32[]{:S(2)}) async-start(bf16[32,8,2048]{2,0,1:T(8,128)(2,1)} %copy.78), calls=%async_computation.2 | async-start | bytes 2097152 | tf_op jit(solution)/shard_map/all_to_all | solution.py:88
  156.9 24.8 %all-to-all-done.1 = bf16[32,8,2048]{2,0,1:T(8,128)(2,1)S(1)} async-done(((bf16[32,8,2048]{2,0,1:T(8,128)(2,1)}), bf16[32,8,2048]{2,0,1:T(8,128)(2,1)S(1)}, u32[]{:S(2)}, u32[]{:S(2)}) %all-to-all-start.1) | async-done | bytes 1048608 | tf_op jit(solution)/shard_map/all_to_all | solution.py:88
  182.4 3.3 %gather_fusion.1 = bf16[512,2048]{1,0:T(8,128)(2,1)} fusion(bf16[257,2048]{1,0:T(8,128)(2,1)S(1)} %concatenate.11, s32[1024]{0:T(1024)S(1)} %pad_clamp_fusion), kind=kCustom, calls=%fused_computation.1 | custom fusion | bytes 4196352 | tf_op jit(solution)/shard_map/jit(_take)/gather | solution.py:108
  185.7 4.4 %gather.15 = bf16[256,2,2048]{2,1,0:T(2,128)(2,1)} reshape(bf16[512,2048]{1,0:T(8,128)(2,1)} %gather_fusion.1) | data formatting | bytes 4194304 | tf_op jit(solution)/shard_map/jit(_take)/gather | solution.py:108
  190.1 10.8 %multiply_reduce_fusion = bf16[256,2048]{1,0:T(8,128)(2,1)} fusion(bf16[256,2,2048]{2,1,0:T(2,128)(2,1)} %gather.15, pred[256,2]{1,0:T(8,128)(4,1)S(1)} %copy.74, f32[256,2]{1,0:T(8,128)S(1)} %copy.81), kind=kLoop, calls=%fused_computation.6 | loop fusion | flops 3670016 | bytes 3148288 | tf_op jit(solution)/shard_map/reduce_sum | solution.py:111
  201.0 2.9 %reduce_sum.62 = bf16[128,2048]{1,0:T(8,128)(2,1)} reduce(bf16[4,128,2048]{2,1,0:T(8,128)(2,1)} %bitcast.48, bf16[]{:T(256)} %constant.72.clone.1), dimensions={0}, to_apply=%region_1.0 | reduce | flops 786432 | bytes 2621442 | tf_op jit(solution)/shard_map/reduce_sum | solution.py:113
  203.9 31.5 %all-reduce.4.cloned.1.call-done = bf16[256,2048]{1,0:T(8,128)(2,1)} async-done(((bf16[256,2048]{1,0:T(8,128)(2,1)}), bf16[256,2048]{1,0:T(8,128)(2,1)}) %all-reduce.4.cloned.1.call-update) | async-done | bytes 1048592 | tf_op jit(solution)/shard_map/psum | solution.py:114
  235.5 2.3 copy.86
  (61 shorter events, 5.8 us)
Async XLA Ops:
  7.2 85.8 %copy-start = (bf16[1,512,2048]{2,1,0:T(8,128)(2,1)S(1)}, bf16[1,512,2048]{2,1,0:T(8,128)(2,1)}, u32[]{:S(2)}) copy-start(bf16[1,512,2048]{2,1,0:T(8,128)(2,1)} %param.27) | copy-start | bytes 6291460
  7.2 5.3 %copy-start.1 = (bf16[256,2048]{1,0:T(8,128)(2,1)S(1)}, bf16[256,2048]{1,0:T(8,128)(2,1)}, u32[]{:S(2)}) copy-start(bf16[256,2048]{1,0:T(8,128)(2,1)} %param.21) | copy-start | bytes 3145732
  7.2 79.2 %all-gather.4.cloned.1.call-start = ((), (), s32[]{:S(2)}) async-start(), calls=%async_computation.3 | async-start | bytes 5242880 | tf_op jit(solution)/shard_map/all_gather | solution.py:77
  52.8 95.0 %reduce-scatter.2.cloned.1.call-start = ((), (), s32[]{:S(2)}) async-start(), calls=%async_computation.4 | async-start | bytes 5242880 | tf_op jit(solution)/shard_map/reduce_scatter | solution.py:82
  103.0 1.0 copy-start.2
  103.0 1.2 copy-start.3
  103.0 6.7 %copy-start.5 = (f32[3,256]{1,0:T(4,128)S(1)}, f32[3,256]{1,0:T(4,128)}, u32[]{:S(2)}) copy-start(f32[3,256]{1,0:T(4,128)} %param.19) | copy-start | bytes 9220
  103.0 98.0 %all-gather.6.cloned.1.call-start = ((), (), s32[]{:S(2)}) async-start(), calls=%async_computation.6 | async-start | bytes 2621440 | tf_op jit(solution)/shard_map/all_gather | solution.py:113
  104.0 1.9 copy-start.7
  106.3 4.7 %collective-permute-start = (bf16[2,256]{1,0:T(2,128)(2,1)S(1)}, bf16[2,256]{1,0:T(2,128)(2,1)S(1)}, u32[]{:S(2)}, u32[]{:S(2)}) collective-permute-start(bf16[2,256]{1,0:T(2,128)(2,1)S(1)} %slice.40), channel_id=1, source_target_pairs={{0,4},{4,8},{8,12},{12,16},{16,20},{20,24},{24,28},{1,5},{5,9},{9,... | collective-permute-start | bytes 3080 | tf_op jit(solution)/shard_map/ppermute | solution.py:10
  147.7 8.7 %copy-start.4 = (s32[256,2]{0,1:T(2,128)S(1)}, s32[256,2]{0,1:T(2,128)}, u32[]{:S(2)}) copy-start(s32[256,2]{0,1:T(2,128)} %param.23) | copy-start | bytes 6148
  147.7 8.9 %copy-start.6 = (f32[256,2]{0,1:T(2,128)S(1)}, f32[256,2]{0,1:T(2,128)}, u32[]{:S(2)}) copy-start(f32[256,2]{0,1:T(2,128)} %param.24) | copy-start | bytes 6148
  150.5 31.2 %all-to-all-start.1 = ((bf16[32,8,2048]{2,0,1:T(8,128)(2,1)}), bf16[32,8,2048]{2,0,1:T(8,128)(2,1)S(1)}, u32[]{:S(2)}, u32[]{:S(2)}) async-start(bf16[32,8,2048]{2,0,1:T(8,128)(2,1)} %copy.78), calls=%async_computation.2 | async-start | bytes 2097152 | tf_op jit(solution)/shard_map/all_to_all | solution.py:88
  156.1 79.4 %all-reduce.4.cloned.1.call-start = ((), (), s32[]{:S(2)}) async-start(), calls=%async_computation.5 | async-start | bytes 2097152 | tf_op jit(solution)/shard_map/psum | solution.py:114
Sparse Core Ops, SparseCore 0:
  52.9 33.4 all-gather.3
  103.1 44.5 reduce-scatter.1
  149.9 22.5 all-gather.5
  201.1 34.3 all-reduce.3
